TPU v7x, 256 devices: a whole 4x4x8 slice. The times are simulated.
256 devices in a mesh: ep: 64 (over z, y, core), tp: 4 (over x).
Axes of the slice: x: 4, y: 4, z: 8, core: 2. Of those that a mesh axis runs over, the one named last changes fastest.
Arguments:
- query_rows: bfloat16 [8192, 1024], P('ep', 'tp'), may hold values from -10 to 10
- key_rows: bfloat16 [8192, 1024], P('ep', 'tp'), may hold values from -10 to 10
- value_rows: bfloat16 [8192, 1024], P('ep', 'tp'), may hold values from -6 to 6
- key_bias: bfloat16 [8192, 16], P('ep', 'tp'), may hold values from -24 to 4
- mixer_weight: bfloat16 [1024, 2048], P('tp'), may hold values from -0.1875 to 0.1875
- mixer_gain: float32 [2048], replicated, may hold values from 0.1 to 1.9
- routed_input: bfloat16 [24576, 2048], P(('ep', 'tp')), may hold values from -6 to 6
- entry_gain: float32 [2048], replicated, may hold values from 0.1 to 1.9
- expert_index: int32 [24576, 2], P(('ep', 'tp')), may hold values from 0 to 127, all different within a row; in each aligned block of 96 rows (0 to 95, 96 to 191, ...) at most 2 rows name the same one
- route_weights: float32 [24576, 2], P(('ep', 'tp')), may hold values from 0.1 to 1
- expert_gate: bfloat16 [128, 2048, 1024], P('ep', None, 'tp'), may hold values from -0.125 to 0.125
- expert_up: bfloat16 [128, 2048, 1024], P('ep', None, 'tp'), may hold values from -0.125 to 0.125
- expert_down: bfloat16 [128, 1024, 2048], P('ep', 'tp'), may hold values from -0.1875 to 0.1875
- shared_gate: bfloat16 [2048, 1024], P(None, 'tp'), may hold values from -0.125 to 0.125
- shared_up: bfloat16 [2048, 1024], P(None, 'tp'), may hold values from -0.125 to 0.125
- shared_down: bfloat16 [1024, 2048], P('tp'), may hold values from -0.1875 to 0.1875
- exit_gain: float32 [2048], replicated, may hold values from 0.1 to 1.9
Outputs:
- mixer_out: bfloat16 [8192, 2048], P(('ep', 'tp'))
- expert_out: bfloat16 [24576, 2048], P(('ep', 'tp'))
Inputs may be any that keep to these rules, and one draw needn't show every extreme that they name: `expert_index`: in each aligned block of 96 rows (the rows of one device) no expert is named by more than 2 rows, a bound that some block reaches; each row names 2 different experts.
All inputs are finite; a program needn't handle non-finite values.
Results may differ from a plain program's by a relative error of at most 0.012.
Values may be sent and summed in bfloat16 or wider, within the bound.
No kernel may reach another device: no remote copies, remote signals or barrier semaphores. Data moves between devices by JAX's collectives and lax.ppermute only.
A program may use at most 128 MiB of HBM per device.

v0:
```python
import jax
import jax.numpy as jnp
from jax import lax
from jax.sharding import PartitionSpec as P

EPS = 1e-06


def in_one_piece(arrays, axis, dim, along):
    widths = [a.shape[along] for a in arrays]
    both = jnp.concatenate(arrays, axis=along)
    filled = lax.all_gather(both, axis, axis=dim, tiled=True)
    return tuple(jnp.split(filled, [sum(widths[:k]) for k in range(1, len(widths))], axis=along))


def in_blocks(array, dim, peers):
    before, after = (array.shape[:dim], array.shape[dim + 1 :])
    return jnp.moveaxis(array.reshape(*before, peers, -1, *after), dim, 0)


def sum_at_owner(array, axis, dim):
    peers = lax.axis_size(axis)
    tiles = lax.all_to_all(in_blocks(array, dim, peers), axis, 0, 0, tiled=True)
    return jnp.sum(tiles.astype(jnp.float32), axis=0)


def root_norm(values, gain_row):
    return values * lax.rsqrt(jnp.mean(values * values, axis=-1, keepdims=True) + EPS) * gain_row


def rounded_term(partial_value):
    return lax.optimization_barrier(partial_value.astype(jnp.bfloat16)).astype(jnp.float32)


def block_shards(shard_rows, ep_size):
    shards = 1
    while shards * shard_rows < 512 and ep_size % (2 * shards) == 0:
        shards = shards * 2
    return shards


def break_scores(query_split, block_keys, block_bias, query_pos, key_start):
    head_count = query_split.shape[1]
    key_count = block_keys.shape[0]
    keys_split = block_keys.reshape(key_count, head_count, query_split.shape[2])
    scores = jnp.einsum("qhd,khd->hqk", query_split, keys_split, preferred_element_type=jnp.float32)
    scores = (
        scores * query_split.shape[2] ** (-0.5)
        + jnp.transpose(block_bias.astype(jnp.float32))[:, None, :]
    )
    key_pos = key_start + jnp.arange(key_count, dtype=jnp.int32)
    causal = (key_pos[None, :] < query_pos[:, None])[None]
    fail_logs = jnp.where(causal, -jax.nn.softplus(scores), 0.0)
    return (scores, fail_logs, causal)


def break_values(scores, fail_logs, causal, offset, block_values):
    later_sum = lax.cumsum(fail_logs, axis=2, reverse=True) - fail_logs + offset[:, :, None]
    weights = jnp.where(causal, jnp.exp(jax.nn.log_sigmoid(scores) + later_sum), 0.0).astype(
        jnp.bfloat16
    )
    values_split = block_values.reshape(block_values.shape[0], scores.shape[0], -1)
    return jnp.einsum("hqk,khd->qhd", weights, values_split, preferred_element_type=jnp.float32)


def shared_term_of(own_all, shared_gate, shared_up, shared_down):
    gate_part = jnp.dot(own_all, shared_gate, preferred_element_type=jnp.float32)
    up_part = jnp.dot(own_all, shared_up, preferred_element_type=jnp.float32)
    hidden = (jax.nn.silu(gate_part) * up_part).astype(jnp.bfloat16)
    return rounded_term(jnp.dot(hidden, shared_down, preferred_element_type=jnp.float32))


def on_device(
    query_rows,
    key_rows,
    value_rows,
    key_bias,
    mixer_weight,
    mixer_gain,
    routed_input,
    entry_gain,
    expert_index,
    route_weights,
    expert_gate,
    expert_up,
    expert_down,
    shared_gate,
    shared_up,
    shared_down,
    exit_gain,
):
    shard_rows = query_rows.shape[0]
    head_count = key_bias.shape[1]
    head_size = query_rows.shape[1] // head_count
    ep_size = lax.axis_size("ep")
    tp_size = lax.axis_size("tp")
    own_index = lax.axis_index("ep")
    query_split = query_rows.reshape(shard_rows, head_count, head_size)
    query_pos = own_index * shard_rows + jnp.arange(shard_rows, dtype=jnp.int32)
    span_shards = block_shards(shard_rows, ep_size)
    empty_output = jnp.zeros((shard_rows, head_count, head_size), jnp.float32)
    all_keys, all_values, all_bias = in_one_piece((key_rows, value_rows, key_bias), "ep", 0, 1)
    block_rows = span_shards * shard_rows
    own_block = own_index * shard_rows // block_rows

    def backward_turn(turn_index, carried_pair):
        output, carried = carried_pair
        block_start = (own_block - turn_index) * block_rows
        block_keys = lax.dynamic_slice_in_dim(all_keys, block_start, block_rows, 0)
        block_values = lax.dynamic_slice_in_dim(all_values, block_start, block_rows, 0)
        block_bias = lax.dynamic_slice_in_dim(all_bias, block_start, block_rows, 0)
        scores, fail_logs, causal = break_scores(
            query_split, block_keys, block_bias, query_pos, block_start
        )
        output = output + break_values(scores, fail_logs, causal, carried, block_values)
        return (output, carried + jnp.sum(fail_logs, axis=2))

    carried_zero = jnp.zeros((head_count, shard_rows), jnp.float32)
    output, unused = lax.fori_loop(0, own_block + 1, backward_turn, (empty_output, carried_zero))
    attended = output.reshape(shard_rows, head_count * head_size).astype(jnp.bfloat16)
    mixer_term = rounded_term(jnp.dot(attended, mixer_weight, preferred_element_type=jnp.float32))
    row_count = routed_input.shape[0]
    top_count = expert_index.shape[1]
    local_experts = expert_gate.shape[0]
    model_width = routed_input.shape[1]
    expert_count = local_experts * ep_size
    capacity = 3 * row_count * top_count // (2 * expert_count)
    slot_total = expert_count * capacity
    normed = root_norm(routed_input.astype(jnp.float32), entry_gain).astype(jnp.bfloat16)
    flat_expert = expert_index.reshape(-1)
    onehot = (flat_expert[:, None] == jnp.arange(expert_count, dtype=jnp.int32)[None, :]).astype(
        jnp.int32
    )
    slot_rank = jnp.sum((jnp.cumsum(onehot, axis=0) - onehot) * onehot, axis=1)
    slot_index = (flat_expert * capacity + slot_rank).reshape(row_count, top_count)
    matches = slot_index[None, :, :] == jnp.arange(slot_total, dtype=jnp.int32)[:, None, None]
    selector = jnp.any(matches, axis=2).astype(jnp.bfloat16)
    outgoing = jnp.dot(selector, normed, preferred_element_type=jnp.float32).astype(jnp.bfloat16)
    outgoing = outgoing.reshape(expert_count, capacity, model_width)
    arrived = lax.all_to_all(outgoing, "ep", split_axis=0, concat_axis=0, tiled=True)
    routed_all, own_all = (
        lax.all_gather(arrived.reshape(slot_total, model_width), "tp", axis=0, tiled=True),
        lax.all_gather(normed, "tp", axis=0, tiled=True),
    )
    routed_split = routed_all.reshape(tp_size, ep_size, local_experts, capacity, model_width)
    gate_part = jnp.einsum(
        "tsecd,edf->tsecf", routed_split, expert_gate, preferred_element_type=jnp.float32
    )
    up_part = jnp.einsum(
        "tsecd,edf->tsecf", routed_split, expert_up, preferred_element_type=jnp.float32
    )
    hidden = (jax.nn.silu(gate_part) * up_part).astype(jnp.bfloat16)
    routed_term = jnp.einsum(
        "tsecf,efd->tsecd", hidden, expert_down, preferred_element_type=jnp.float32
    )
    routed_term = rounded_term(routed_term.reshape(tp_size * slot_total, model_width))
    shared_term = shared_term_of(own_all, shared_gate, shared_up, shared_down)
    mixer_sum, routed_sum, shared_sum = (
        sum_at_owner(mixer_term.astype(jnp.bfloat16), "tp", 0),
        sum_at_owner(routed_term.astype(jnp.bfloat16), "tp", 0),
        sum_at_owner(shared_term.astype(jnp.bfloat16), "tp", 0),
    )
    returned_rows = routed_sum.astype(jnp.bfloat16).reshape(expert_count, capacity, model_width)
    back_rows = lax.all_to_all(
        returned_rows, "ep", split_axis=0, concat_axis=0, tiled=True
    ).reshape(slot_total, model_width)
    gathered = back_rows[slot_index].astype(jnp.float32)
    routed = jnp.sum(route_weights[:, :, None] * gathered, axis=1)
    combined = routed + shared_sum
    expert_out = root_norm(combined, exit_gain).astype(jnp.bfloat16)
    mixer_out = root_norm(mixer_sum, mixer_gain).astype(jnp.bfloat16)
    return (mixer_out, expert_out)


def solution(mesh):
    in_specs = (
        P("ep", "tp"),
        P("ep", "tp"),
        P("ep", "tp"),
        P("ep", "tp"),
        P("tp", None),
        P(),
        P(("ep", "tp"), None),
        P(),
        P(("ep", "tp"), None),
        P(("ep", "tp"), None),
        P("ep", None, "tp"),
        P("ep", None, "tp"),
        P("ep", "tp", None),
        P(None, "tp"),
        P(None, "tp"),
        P("tp", None),
        P(),
    )
    out_specs = (P(("ep", "tp"), None), P(("ep", "tp"), None))
    return jax.shard_map(
        on_device, mesh=mesh, in_specs=in_specs, out_specs=out_specs, check_vma=False
    )
```

profile of v0, /device:TPU:248, one launch (start us, length us, event | category | flops | bytes accessed | tf_op | source)
XLA Modules:
  0.0 446.3 jit_solution(14355067020275289579)
XLA Ops:
  15.6 34.0 %all_to_all.25 = bf16[128,2,2048]{2,1,0:T(2,128)(2,1)S(1)} all-to-all(bf16[128,2,2048]{2,1,0:T(2,128)(2,1)} %reshape.136), channel_id=1, replica_groups=mesh['ep'=64,'tp'=4] {'ep'}, dimensions={0} | all-to-all | bytes 2097152 | tf_op jit(solution)/shard_map/all_to_all | solution.py:140
  54.3 48.0 %all-gather.6.cloned.1.call-done = bf16[1024,2048]{1,0:T(8,128)(2,1)} async-done(((bf16[256,2048]{1,0:T(8,128)(2,1)}), bf16[1024,2048]{1,0:T(8,128)(2,1)}) %all-gather.6.cloned.1.call-update) | async-done | bytes 4194320 | tf_op jit(solution)/shard_map/all_gather | solution.py:142
  102.3 8.1 %reshape.138 = bf16[4,64,2,2,2048]{4,3,2,1,0:T(2,128)(2,1)} reshape(bf16[1024,2048]{1,0:T(8,128)(2,1)} %all-gather.6.cloned.1.call-done) | data formatting | bytes 8388608 | tf_op jit(solution)/shard_map/reshape | solution.py:145
  110.4 7.4 %fusion.23 = f32[4,64,2,2,256]{4,1,3,0,2:T(8,128)S(1)} fusion(bf16[2,2048,256]{2,1,0:T(8,128)(2,1)} %param.29, bf16[4,64,2,2,2048]{4,3,2,1,0:T(2,128)(2,1)} %reshape.138), kind=kOutput, calls=%fused_computation.42 | convolution fusion | flops 1073741824 | bytes 7340032 | tf_op jit(solution)/shard_map/tsecd,edf->tsecf/dot_general | solution.py:146
  117.9 10.8 %convert_bitcast_fusion.1 = bf16[4,64,2,2,2048]{4,1,3,0,2:T(8,128)(2,1)} fusion(bf16[2,256,2048]{2,1,0:T(8,128)(2,1)S(1)} %copy-done, bf16[2,2048,256]{2,1,0:T(8,128)(2,1)} %param.30, bf16[4,64,2,2,2048]{4,3,2,1,0:T(2,128)(2,1)} %reshape.138, f32[4,64,2,2,256]{4,1,3,0,2:T(8,128)S(1)} %fusion.23), kind=kOutput, calls=%fused_computation.29 | convolution fusion | flops 2151153664 | bytes 13631488 | tf_op jit(solution)/shard_map/tsecf,efd->tsecd/dot_general | solution.py:153
  128.6 8.7 %copy.70 = bf16[4,64,2,2,2048]{4,3,2,1,0:T(2,128)(2,1)} copy(bf16[4,64,2,2,2048]{4,1,3,0,2:T(8,128)(2,1)} %convert_bitcast_fusion.1) | data formatting | bytes 8388608 | tf_op jit(solution)/shard_map/convert_element_type | solution.py:32
  137.4 7.2 %convert_element_type.80 = bf16[1024,2048]{1,0:T(8,128)(2,1)} reshape(bf16[4,64,2,2,2048]{4,3,2,1,0:T(2,128)(2,1)} %copy.70) | data formatting | bytes 8388608 | tf_op jit(solution)/shard_map/convert_element_type | solution.py:32
  144.6 5.0 %all-to-all-start.2 = ((bf16[4,256,2048]{2,1,0:T(8,128)(2,1)}), bf16[4,256,2048]{2,1,0:T(8,128)(2,1)}, u32[]{:S(2)}, u32[]{:S(2)}) async-start(bf16[4,256,2048]{2,1,0:T(8,128)(2,1)} %bitcast.107), calls=%async_computation.2 | async-start | bytes 8388608 | tf_op jit(solution)/shard_map/all_to_all | solution.py:23
  156.3 42.4 %all-to-all-done.2 = bf16[4,256,2048]{2,1,0:T(8,128)(2,1)} async-done(((bf16[4,256,2048]{2,1,0:T(8,128)(2,1)}), bf16[4,256,2048]{2,1,0:T(8,128)(2,1)}, u32[]{:S(2)}, u32[]{:S(2)}) %all-to-all-start.2) | async-done | bytes 4194336 | tf_op jit(solution)/shard_map/all_to_all | solution.py:23
  207.0 15.3 %all-to-all-done.4 = bf16[4,96,2048]{2,1,0:T(8,128)(2,1)S(1)} async-done(((bf16[4,96,2048]{2,1,0:T(8,128)(2,1)}), bf16[4,96,2048]{2,1,0:T(8,128)(2,1)S(1)}, u32[]{:S(2)}, u32[]{:S(2)}) %all-to-all-start.4) | async-done | bytes 1572896 | tf_op jit(solution)/shard_map/all_to_all | solution.py:23
  222.2 10.5 %all-to-all-start.3 = ((bf16[128,2,2048]{2,1,0:T(2,128)(2,1)}), bf16[128,2,2048]{2,1,0:T(2,128)(2,1)S(1)}, u32[]{:S(2)}, u32[]{:S(2)}) async-start(bf16[128,2,2048]{2,1,0:T(2,128)(2,1)} %reshape.140), calls=%async_computation.3 | async-start | bytes 2097152 | tf_op jit(solution)/shard_map/all_to_all | solution.py:164
  234.4 23.3 %all-to-all-done.3 = bf16[128,2,2048]{2,1,0:T(2,128)(2,1)S(1)} async-done(((bf16[128,2,2048]{2,1,0:T(2,128)(2,1)}), bf16[128,2,2048]{2,1,0:T(2,128)(2,1)S(1)}, u32[]{:S(2)}, u32[]{:S(2)}) %all-to-all-start.3) | async-done | bytes 1048608 | tf_op jit(solution)/shard_map/all_to_all | solution.py:164
  265.9 5.9 %fusion.68 = (bf16[8192,256]{0,1:T(8,128)(2,1)}, bf16[8192,256]{0,1:T(8,128)(2,1)}) fusion(bf16[8192,516]{0,1:T(8,128)(2,1)} %all-gather.4.cloned.1.call-done), kind=kLoop, calls=%fused_computation.89 | loop fusion | bytes 16777216 | tf_op jit(solution)/shard_map/split | solution.py:13
  271.8 150.8 %while.13 = (s32[]{:T(128)}, f32[128,4,64]{0,2,1:T(8,128)S(1)}, f32[4,128]{1,0:T(4,128)S(1)}, s32[]{:T(128)}, s32[]{:T(128)}, /*index=5*/bf16[8192,256]{0,1:T(8,...) while((s32[]{:T(128)}, f32[128,4,64]{0,2,1:T(8,128)S(1)}, ...), condition=%wide.region_4.5_spmd.clone, body=%wide.region_0.4_spmd.clone.sunk | while | flops 109160584 | bytes 13726939 | solution.py:119
  274.3 4.8 %fusion.98 = f32[4,128,4,128]{1,2,3,0:T(4,128)S(1)} fusion(f32[4,128,4,128]{1,3,2,0:T(8,128)S(1)} %bitcast.105), kind=kOutput, calls=%fused_computation.18.clone.1 | output fusion | flops 33292288 | bytes 2097152 | tf_op jit(solution)/shard_map/reduce-window
  283.7 4.8 %fusion.98 = f32[4,128,4,128]{1,2,3,0:T(4,128)S(1)} fusion(f32[4,128,4,128]{1,3,2,0:T(8,128)S(1)} %bitcast.105), kind=kOutput, calls=%fused_computation.18.clone.1 | output fusion | flops 33292288 | bytes 2097152 | tf_op jit(solution)/shard_map/reduce-window
  293.1 4.8 %fusion.98 = f32[4,128,4,128]{1,2,3,0:T(4,128)S(1)} fusion(f32[4,128,4,128]{1,3,2,0:T(8,128)S(1)} %bitcast.105), kind=kOutput, calls=%fused_computation.18.clone.1 | output fusion | flops 33292288 | bytes 2097152 | tf_op jit(solution)/shard_map/reduce-window
  302.6 4.8 %fusion.98 = f32[4,128,4,128]{1,2,3,0:T(4,128)S(1)} fusion(f32[4,128,4,128]{1,3,2,0:T(8,128)S(1)} %bitcast.105), kind=kOutput, calls=%fused_computation.18.clone.1 | output fusion | flops 33292288 | bytes 2097152 | tf_op jit(solution)/shard_map/reduce-window
  312.0 4.8 %fusion.98 = f32[4,128,4,128]{1,2,3,0:T(4,128)S(1)} fusion(f32[4,128,4,128]{1,3,2,0:T(8,128)S(1)} %bitcast.105), kind=kOutput, calls=%fused_computation.18.clone.1 | output fusion | flops 33292288 | bytes 2097152 | tf_op jit(solution)/shard_map/reduce-window
  321.4 4.8 %fusion.98 = f32[4,128,4,128]{1,2,3,0:T(4,128)S(1)} fusion(f32[4,128,4,128]{1,3,2,0:T(8,128)S(1)} %bitcast.105), kind=kOutput, calls=%fused_computation.18.clone.1 | output fusion | flops 33292288 | bytes 2097152 | tf_op jit(solution)/shard_map/reduce-window
  330.8 4.8 %fusion.98 = f32[4,128,4,128]{1,2,3,0:T(4,128)S(1)} fusion(f32[4,128,4,128]{1,3,2,0:T(8,128)S(1)} %bitcast.105), kind=kOutput, calls=%fused_computation.18.clone.1 | output fusion | flops 33292288 | bytes 2097152 | tf_op jit(solution)/shard_map/reduce-window
  368.5 4.8 %fusion.98 = f32[4,128,4,128]{1,2,3,0:T(4,128)S(1)} fusion(f32[4,128,4,128]{1,3,2,0:T(8,128)S(1)} %bitcast.105), kind=kOutput, calls=%fused_computation.18.clone.1 | output fusion | flops 33292288 | bytes 2097152 | tf_op jit(solution)/shard_map/reduce-window
  377.9 4.8 %fusion.98 = f32[4,128,4,128]{1,2,3,0:T(4,128)S(1)} fusion(f32[4,128,4,128]{1,3,2,0:T(8,128)S(1)} %bitcast.105), kind=kOutput, calls=%fused_computation.18.clone.1 | output fusion | flops 33292288 | bytes 2097152 | tf_op jit(solution)/shard_map/reduce-window
  429.5 9.1 %all-to-all-done = bf16[4,32,2048]{2,1,0:T(8,128)(2,1)S(1)} async-done(((bf16[4,32,2048]{2,1,0:T(8,128)(2,1)}), bf16[4,32,2048]{2,1,0:T(8,128)(2,1)S(1)}, u32[]{:S(2)}, u32[]{:S(2)}) %all-to-all-start) | async-done | bytes 524320 | tf_op jit(solution)/shard_map/all_to_all | solution.py:23
  (317 shorter events, 151.2 us)
Async XLA Ops:
  7.2 110.7 %copy-start = (bf16[2,256,2048]{2,1,0:T(8,128)(2,1)S(1)}, bf16[2,256,2048]{2,1,0:T(8,128)(2,1)}, u32[]{:S(2)}) copy-start(bf16[2,256,2048]{2,1,0:T(8,128)(2,1)} %param.31) | copy-start | bytes 6291460
  7.2 95.1 %all-gather.6.cloned.1.call-start = ((), (), s32[]{:S(2)}) async-start(), calls=%async_computation.6 | async-start | bytes 5242880 | tf_op jit(solution)/shard_map/all_gather | solution.py:142
  12.8 36.8 %copy-start.2 = (bf16[96,2048]{1,0:T(8,128)(2,1)}, bf16[96,2048]{1,0:T(8,128)(2,1)S(1)}, u32[]{:S(2)}) copy-start(bf16[96,2048]{1,0:T(8,128)(2,1)S(1)} %fusion.53) | copy-start | bytes 1179652
  49.6 4.0 copy-start.8
  50.9 98.8 %all-gather.8.cloned.1.call-start = ((), (), s32[]{:S(2)}) async-start(), calls=%async_computation.7 | async-start | bytes 1966080 | tf_op jit(solution)/shard_map/all_gather | solution.py:143
  51.6 214.2 %all-gather.4.cloned.1.call-start = ((), (), s32[]{:S(2)}) async-start(), calls=%async_computation.5 | async-start | bytes 8652800 | tf_op jit(solution)/shard_map/all_gather | solution.py:12
  144.6 5.1 %copy-start.11 = (bf16[2048,256]{1,0:T(8,128)(2,1)S(1)}, bf16[2048,256]{1,0:T(8,128)(2,1)}, u32[]{:S(2)}) copy-start(bf16[2048,256]{1,0:T(8,128)(2,1)} %param.32) | copy-start | bytes 3145732
  144.6 54.1 %all-to-all-start.2 = ((bf16[4,256,2048]{2,1,0:T(8,128)(2,1)}), bf16[4,256,2048]{2,1,0:T(8,128)(2,1)}, u32[]{:S(2)}, u32[]{:S(2)}) async-start(bf16[4,256,2048]{2,1,0:T(8,128)(2,1)} %bitcast.107), calls=%async_computation.2 | async-start | bytes 8388608 | tf_op jit(solution)/shard_map/all_to_all | solution.py:23
  149.7 2.1 copy-start.10
  198.7 23.6 %all-to-all-start.4 = ((bf16[4,96,2048]{2,1,0:T(8,128)(2,1)}), bf16[4,96,2048]{2,1,0:T(8,128)(2,1)S(1)}, u32[]{:S(2)}, u32[]{:S(2)}) async-start(bf16[4,96,2048]{2,1,0:T(8,128)(2,1)} %bitcast.109), calls=%async_computation.4 | async-start | bytes 3145728 | tf_op jit(solution)/shard_map/all_to_all | solution.py:23
  205.4 27.4 %copy-start.5 = (bf16[128,256]{1,0:T(8,128)(2,1)S(1)}, bf16[128,256]{1,0:T(8,128)(2,1)}, u32[]{:S(2)}) copy-start(bf16[128,256]{1,0:T(8,128)(2,1)} %param.19) | copy-start | bytes 196612
  205.4 27.7 %copy-start.9 = (f32[96,2]{0,1:T(2,128)S(1)}, f32[96,2]{0,1:T(2,128)}, u32[]{:S(2)}) copy-start(f32[96,2]{0,1:T(2,128)} %param.28) | copy-start | bytes 2308
  222.2 35.4 %all-to-all-start.3 = ((bf16[128,2,2048]{2,1,0:T(2,128)(2,1)}), bf16[128,2,2048]{2,1,0:T(2,128)(2,1)S(1)}, u32[]{:S(2)}, u32[]{:S(2)}) async-start(bf16[128,2,2048]{2,1,0:T(2,128)(2,1)} %reshape.140), calls=%async_computation.3 | async-start | bytes 2097152 | tf_op jit(solution)/shard_map/all_to_all | solution.py:164
  260.2 4.5 %copy-start.4 = (f32[96,2048]{1,0:T(8,128)S(1)}, f32[96,2048]{1,0:T(8,128)}, u32[]{:S(2)}) copy-start(f32[96,2048]{1,0:T(8,128)} %convert_reduce_fusion) | copy-start | bytes 2359300
  265.8 5.9 %slice-start = ((bf16[8192,516]{0,1:T(8,128)(2,1)}), bf16[8192,4]{0,1:T(4,128)(2,1)S(1)}, s32[]{:S(2)}) async-start(bf16[8192,516]{0,1:T(8,128)(2,1)} %all-gather.4.cloned.1.call-done), calls=%async_computation.8 | async-start | bytes 131072 | tf_op jit(solution)/shard_map/split | solution.py:13
  422.6 6.0 %copy-start.3 = (f32[96,2048]{1,0:T(8,128)S(1)}, f32[96,2048]{1,0:T(8,128)}, u32[]{:S(2)}) copy-start(f32[96,2048]{1,0:T(8,128)} %get-tuple-element.101) | copy-start | bytes 2359300
  422.6 6.0 %copy-start.6 = (f32[2048]{0:T(1024)S(1)}, f32[2048]{0:T(1024)}, u32[]{:S(2)}) copy-start(f32[2048]{0:T(1024)} %param.35) | copy-start | bytes 24580
  422.6 16.2 %copy-start.7 = (f32[2048]{0:T(1024)S(1)}, f32[2048]{0:T(1024)}, u32[]{:S(2)}) copy-start(f32[2048]{0:T(1024)} %param.24) | copy-start | bytes 24580
  422.6 17.0 %copy-start.1 = (bf16[2,256,2048]{2,1,0:T(8,128)(2,1)S(1)}, bf16[2,256,2048]{2,1,0:T(8,128)(2,1)}, u32[]{:S(2)}) copy-start(bf16[2,256,2048]{2,1,0:T(8,128)(2,1)} %param.31) | copy-start | bytes 6291460
  425.1 13.5 %all-to-all-start = ((bf16[4,32,2048]{2,1,0:T(8,128)(2,1)}), bf16[4,32,2048]{2,1,0:T(8,128)(2,1)S(1)}, u32[]{:S(2)}, u32[]{:S(2)}) async-start(bf16[4,32,2048]{2,1,0:T(8,128)(2,1)} %bitcast.2), calls=%async_computation | async-start | bytes 1048576 | tf_op jit(solution)/shard_map/all_to_all | solution.py:23
Sparse Core Ops, SparseCore 0:
  51.0 51.2 all-gather.5
  104.7 29.3 all-gather.7
  136.7 85.6 all-gather.3
where the time goes:
time: 451 us; the launch traced here: 446 us
  waiting for transfers between devices  139 us (31%)
  other arithmetic  121 us (27%)
  local copies, waits for them, and re-layouts  61.9 us (14%)
  matrix products  51.6 us (11%)
  blocking collectives  34 us (8%)
  starting transfers between devices  22.7 us (5%)
  between operations  14.4 us (3%)
    another operation x36, other arithmetic  77.5 us
    all_to_all x3, waiting for transfers between devices, sum_at_owner(): tiles = lax.all_to_all(in_blocks(array, dim, peers), axis, 0, 0, tiled=True)  66.8 us
    all_gather x1, waiting for transfers between devices, on_device(): lax.all_gather(arrived.reshape(slot_total, model_width), 'tp', axis=0, ti...  48 us
    all_to_all x1, blocking collectives, on_device(): lax.all_to_all(outgoing, 'ep', split_axis=0, concat_axis=0, tiled=True)  34 us
    convert_element_type x16, other arithmetic, break_values(): jnp.where(causal, jnp.exp(jax.nn.log_sigmoid(scores) + later_sum), 0.0)  23.7 us
    all_to_all x1, waiting for transfers between devices, on_device(): lax.all_to_all(returned_rows, 'ep', split_axis=0, concat_axis=0, tiled=True)  23.3 us
    dot_general x16, matrix products, break_scores(): jnp.einsum('qhd,khd->hqk', query_split, keys_split, preferred_element_typ...  19.5 us
    dynamic_slice x16, local copies, waits for them, and re-layouts, backward_turn(): block_keys = lax.dynamic_slice_in_dim(all_keys, block_start, block_rows, 0)  17.1 us
  transfers between devices with their start and end apart: 7, of which 5 were waited for; matrix products, arithmetic and copies ran while one was open for 15% of the time, Pallas kernels for 0%

commit v1 on v0

--- a/solution.py
+++ b/solution.py
@@ -4,6 +4,14 @@
 from jax.sharding import PartitionSpec as P
 
 EPS = 1e-06
+
+
+def gather_from_all(value, axis, dim):
+    count = lax.axis_size(axis)
+    repeats = [count if d == dim else 1 for d in range(value.ndim)]
+    return lax.all_to_all(
+        jnp.tile(value, repeats), axis, split_axis=dim, concat_axis=dim, tiled=True
+    )
 
 
 def in_one_piece(arrays, axis, dim, along):
@@ -139,7 +147,7 @@
     outgoing = outgoing.reshape(expert_count, capacity, model_width)
     arrived = lax.all_to_all(outgoing, "ep", split_axis=0, concat_axis=0, tiled=True)
     routed_all, own_all = (
-        lax.all_gather(arrived.reshape(slot_total, model_width), "tp", axis=0, tiled=True),
+        gather_from_all(arrived.reshape(slot_total, model_width), "tp", 0),
         lax.all_gather(normed, "tp", axis=0, tiled=True),
     )
     routed_split = routed_all.reshape(tp_size, ep_size, local_experts, capacity, model_width)

time: 451 us -> 447 us (level)
  blocking collectives: 34 us -> 87.3 us
  waiting for transfers between devices: 139 us -> 88 us
    all_to_all x0 -> x1, blocking collectives: none -> 53.2 us  [gather_from_all(): lax.all_to_all(jnp.tile(value, repeats), axis, split_axis=dim, concat_axi...]
    all_gather x1 -> x0, waiting for transfers between devices: 48 us -> none  [on_device(): lax.all_gather(arrived.reshape(slot_total, model_width), 'tp', axis=0, ti...]
    reshape x2 -> x0, local copies, waits for them, and re-layouts: 9.34 us -> none  [the longest x1 8.11 us: on_device(): routed_all.reshape(tp_size, ep_size, local_experts, capacity, model_width)]
  transfers between devices with their start and end apart: 7 -> 6, of which waited for: 5 -> 4; matrix products, arithmetic and copies ran while one was open for 15% -> 15% of each run, Pallas kernels for 0% -> 0%
where the time goes in v1:
time: 447 us; the launch traced here: 442 us
  other arithmetic  121 us (27%)
  waiting for transfers between devices  88 us (20%)
  blocking collectives  87.3 us (20%)
  local copies, waits for them, and re-layouts  58.7 us (13%)
  matrix products  48.3 us (11%)
  starting transfers between devices  22.3 us (5%)
  between operations  14.7 us (3%)
    another operation x36, other arithmetic  77.5 us
    all_to_all x3, waiting for transfers between devices, sum_at_owner(): tiles = lax.all_to_all(in_blocks(array, dim, peers), axis, 0, 0, tiled=True)  64.7 us
    all_to_all x1, blocking collectives, gather_from_all(): lax.all_to_all(jnp.tile(value, repeats), axis, split_axis=dim, concat_axi...  53.2 us
    all_to_all x1, blocking collectives, on_device(): lax.all_to_all(outgoing, 'ep', split_axis=0, concat_axis=0, tiled=True)  34.1 us
    convert_element_type x16, other arithmetic, break_values(): jnp.where(causal, jnp.exp(jax.nn.log_sigmoid(scores) + later_sum), 0.0)  23.7 us
    all_to_all x1, waiting for transfers between devices, on_device(): lax.all_to_all(returned_rows, 'ep', split_axis=0, concat_axis=0, tiled=True)  23.3 us
    dot_general x16, matrix products, break_scores(): jnp.einsum('qhd,khd->hqk', query_split, keys_split, preferred_element_typ...  19.5 us
    dynamic_slice x16, local copies, waits for them, and re-layouts, backward_turn(): block_keys = lax.dynamic_slice_in_dim(all_keys, block_start, block_rows, 0)  17.1 us
  transfers between devices with their start and end apart: 6, of which 4 were waited for; matrix products, arithmetic and copies ran while one was open for 15% of the time, Pallas kernels for 0%

profile of v1, /device:TPU:248, one launch (start us, length us, event | category | flops | bytes accessed | tf_op | source)
XLA Modules:
  0.0 442.5 jit_solution(14837349370967075856)
XLA Ops:
  17.1 34.1 %all_to_all.31 = bf16[128,2,2048]{2,1,0:T(2,128)(2,1)} all-to-all(bf16[128,2,2048]{2,1,0:T(2,128)(2,1)} %reshape.141), channel_id=1, replica_groups=mesh['ep'=64,'tp'=4] {'ep'}, dimensions={0} | all-to-all | bytes 2097152 | tf_op jit(solution)/shard_map/all_to_all | solution.py:148
  53.2 53.2 %all_to_all.32 = bf16[4,256,2048]{2,1,0:T(8,128)(2,1)S(1)} all-to-all(bf16[4,256,2048]{2,1,0:T(8,128)(2,1)S(1)} %tile.9), channel_id=1, replica_groups=mesh['ep'=64,'tp'=4] {'tp'}, dimensions={0} | all-to-all | bytes 8388608 | tf_op jit(solution)/shard_map/all_to_all | solution.py:12
  116.1 11.1 %convert_bitcast_fusion.1 = bf16[4,64,2,2,2048]{4,1,3,0,2:T(8,128)(2,1)} fusion(bf16[2,256,2048]{2,1,0:T(8,128)(2,1)S(1)} %copy-done, bf16[2,2048,256]{2,1,0:T(8,128)(2,1)} %param.30, bf16[4,64,2,2,2048]{4,0,3,2,1:T(4,128)(2,1)} %bitcast.111, f32[4,64,2,2,256]{4,1,3,0,2:T(8,128)S(1)} %fusion.23), kind=kOutput, calls=%fused_computation.29 | convolution fusion | flops 2151153664 | bytes 13631488 | tf_op jit(solution)/shard_map/tsecf,efd->tsecd/dot_general | solution.py:161
  127.2 8.5 %copy.88 = bf16[4,64,2,2,2048]{4,3,2,1,0:T(2,128)(2,1)} copy(bf16[4,64,2,2,2048]{4,1,3,0,2:T(8,128)(2,1)} %convert_bitcast_fusion.1) | data formatting | bytes 8388608 | tf_op jit(solution)/shard_map/convert_element_type | solution.py:40
  135.7 7.2 %convert_element_type.80 = bf16[1024,2048]{1,0:T(8,128)(2,1)} reshape(bf16[4,64,2,2,2048]{4,3,2,1,0:T(2,128)(2,1)} %copy.88) | data formatting | bytes 8388608 | tf_op jit(solution)/shard_map/convert_element_type | solution.py:40
  142.9 5.0 %all-to-all-start.3 = ((bf16[4,256,2048]{2,1,0:T(8,128)(2,1)}), bf16[4,256,2048]{2,1,0:T(8,128)(2,1)}, u32[]{:S(2)}, u32[]{:S(2)}) async-start(bf16[4,256,2048]{2,1,0:T(8,128)(2,1)} %bitcast.108), calls=%async_computation.3 | async-start | bytes 8388608 | tf_op jit(solution)/shard_map/all_to_all | solution.py:31
  154.6 41.3 %all-to-all-done.3 = bf16[4,256,2048]{2,1,0:T(8,128)(2,1)} async-done(((bf16[4,256,2048]{2,1,0:T(8,128)(2,1)}), bf16[4,256,2048]{2,1,0:T(8,128)(2,1)}, u32[]{:S(2)}, u32[]{:S(2)}) %all-to-all-start.3) | async-done | bytes 4194336 | tf_op jit(solution)/shard_map/all_to_all | solution.py:31
  204.1 14.3 %all-to-all-done.5 = bf16[4,96,2048]{2,1,0:T(8,128)(2,1)S(1)} async-done(((bf16[4,96,2048]{2,1,0:T(8,128)(2,1)}), bf16[4,96,2048]{2,1,0:T(8,128)(2,1)S(1)}, u32[]{:S(2)}, u32[]{:S(2)}) %all-to-all-start.5) | async-done | bytes 1572896 | tf_op jit(solution)/shard_map/all_to_all | solution.py:31
  218.4 10.2 %all-to-all-start.4 = ((bf16[128,2,2048]{2,1,0:T(2,128)(2,1)}), bf16[128,2,2048]{2,1,0:T(2,128)(2,1)S(1)}, u32[]{:S(2)}, u32[]{:S(2)}) async-start(bf16[128,2,2048]{2,1,0:T(2,128)(2,1)} %reshape.144), calls=%async_computation.4 | async-start | bytes 2097152 | tf_op jit(solution)/shard_map/all_to_all | solution.py:172
  230.2 23.3 %all-to-all-done.4 = bf16[128,2,2048]{2,1,0:T(2,128)(2,1)S(1)} async-done(((bf16[128,2,2048]{2,1,0:T(2,128)(2,1)}), bf16[128,2,2048]{2,1,0:T(2,128)(2,1)S(1)}, u32[]{:S(2)}, u32[]{:S(2)}) %all-to-all-start.4) | async-done | bytes 1048608 | tf_op jit(solution)/shard_map/all_to_all | solution.py:172
  261.7 5.9 %fusion.69 = (bf16[8192,256]{0,1:T(8,128)(2,1)}, bf16[8192,256]{0,1:T(8,128)(2,1)}) fusion(bf16[8192,516]{0,1:T(8,128)(2,1)} %all-gather.3.cloned.1.call-done), kind=kLoop, calls=%fused_computation.90 | loop fusion | bytes 16777216 | tf_op jit(solution)/shard_map/split | solution.py:21
  267.6 150.8 %while.13 = (s32[]{:T(128)}, f32[128,4,64]{0,2,1:T(8,128)S(1)}, f32[4,128]{1,0:T(4,128)S(1)}, s32[]{:T(128)}, s32[]{:T(128)}, /*index=5*/bf16[8192,256]{0,1:T(8,...) while((s32[]{:T(128)}, f32[128,4,64]{0,2,1:T(8,128)S(1)}, ...), condition=%wide.region_4.5_spmd.clone, body=%wide.region_0.4_spmd.clone.sunk | while | flops 109160584 | bytes 13726939 | solution.py:127
  270.1 4.8 %fusion.99 = f32[4,128,4,128]{1,2,3,0:T(4,128)S(1)} fusion(f32[4,128,4,128]{1,3,2,0:T(8,128)S(1)} %bitcast.106), kind=kOutput, calls=%fused_computation.18.clone.1 | output fusion | flops 33292288 | bytes 2097152 | tf_op jit(solution)/shard_map/reduce-window
  279.5 4.8 %fusion.99 = f32[4,128,4,128]{1,2,3,0:T(4,128)S(1)} fusion(f32[4,128,4,128]{1,3,2,0:T(8,128)S(1)} %bitcast.106), kind=kOutput, calls=%fused_computation.18.clone.1 | output fusion | flops 33292288 | bytes 2097152 | tf_op jit(solution)/shard_map/reduce-window
  289.0 4.8 %fusion.99 = f32[4,128,4,128]{1,2,3,0:T(4,128)S(1)} fusion(f32[4,128,4,128]{1,3,2,0:T(8,128)S(1)} %bitcast.106), kind=kOutput, calls=%fused_computation.18.clone.1 | output fusion | flops 33292288 | bytes 2097152 | tf_op jit(solution)/shard_map/reduce-window
  298.4 4.8 %fusion.99 = f32[4,128,4,128]{1,2,3,0:T(4,128)S(1)} fusion(f32[4,128,4,128]{1,3,2,0:T(8,128)S(1)} %bitcast.106), kind=kOutput, calls=%fused_computation.18.clone.1 | output fusion | flops 33292288 | bytes 2097152 | tf_op jit(solution)/shard_map/reduce-window
  307.8 4.8 %fusion.99 = f32[4,128,4,128]{1,2,3,0:T(4,128)S(1)} fusion(f32[4,128,4,128]{1,3,2,0:T(8,128)S(1)} %bitcast.106), kind=kOutput, calls=%fused_computation.18.clone.1 | output fusion | flops 33292288 | bytes 2097152 | tf_op jit(solution)/shard_map/reduce-window
  317.2 4.8 %fusion.99 = f32[4,128,4,128]{1,2,3,0:T(4,128)S(1)} fusion(f32[4,128,4,128]{1,3,2,0:T(8,128)S(1)} %bitcast.106), kind=kOutput, calls=%fused_computation.18.clone.1 | output fusion | flops 33292288 | bytes 2097152 | tf_op jit(solution)/shard_map/reduce-window
  326.7 4.8 %fusion.99 = f32[4,128,4,128]{1,2,3,0:T(4,128)S(1)} fusion(f32[4,128,4,128]{1,3,2,0:T(8,128)S(1)} %bitcast.106), kind=kOutput, calls=%fused_computation.18.clone.1 | output fusion | flops 33292288 | bytes 2097152 | tf_op jit(solution)/shard_map/reduce-window
  336.1 4.8 %fusion.99 = f32[4,128,4,128]{1,2,3,0:T(4,128)S(1)} fusion(f32[4,128,4,128]{1,3,2,0:T(8,128)S(1)} %bitcast.106), kind=kOutput, calls=%fused_computation.18.clone.1 | output fusion | flops 33292288 | bytes 2097152 | tf_op jit(solution)/shard_map/reduce-window
  345.5 4.8 %fusion.99 = f32[4,128,4,128]{1,2,3,0:T(4,128)S(1)} fusion(f32[4,128,4,128]{1,3,2,0:T(8,128)S(1)} %bitcast.106), kind=kOutput, calls=%fused_computation.18.clone.1 | output fusion | flops 33292288 | bytes 2097152 | tf_op jit(solution)/shard_map/reduce-window
  354.9 4.8 %fusion.99 = f32[4,128,4,128]{1,2,3,0:T(4,128)S(1)} fusion(f32[4,128,4,128]{1,3,2,0:T(8,128)S(1)} %bitcast.106), kind=kOutput, calls=%fused_computation.18.clone.1 | output fusion | flops 33292288 | bytes 2097152 | tf_op jit(solution)/shard_map/reduce-window
  364.3 4.8 %fusion.99 = f32[4,128,4,128]{1,2,3,0:T(4,128)S(1)} fusion(f32[4,128,4,128]{1,3,2,0:T(8,128)S(1)} %bitcast.106), kind=kOutput, calls=%fused_computation.18.clone.1 | output fusion | flops 33292288 | bytes 2097152 | tf_op jit(solution)/shard_map/reduce-window
  425.3 9.1 %all-to-all-done = bf16[4,32,2048]{2,1,0:T(8,128)(2,1)S(1)} async-done(((bf16[4,32,2048]{2,1,0:T(8,128)(2,1)}), bf16[4,32,2048]{2,1,0:T(8,128)(2,1)S(1)}, u32[]{:S(2)}, u32[]{:S(2)}) %all-to-all-start) | async-done | bytes 524320 | tf_op jit(solution)/shard_map/all_to_all | solution.py:31
  (320 shorter events, 150.1 us)
Async XLA Ops:
  7.2 109.0 %copy-start = (bf16[2,256,2048]{2,1,0:T(8,128)(2,1)S(1)}, bf16[2,256,2048]{2,1,0:T(8,128)(2,1)}, u32[]{:S(2)}) copy-start(bf16[2,256,2048]{2,1,0:T(8,128)(2,1)} %param.31) | copy-start | bytes 6291460
  7.2 6.7 %copy-start.9 = (s32[96,2]{0,1:T(2,128)S(1)}, s32[96,2]{0,1:T(2,128)}, u32[]{:S(2)}) copy-start(s32[96,2]{0,1:T(2,128)} %param.27) | copy-start | bytes 2308
  7.2 140.8 %all-gather.5.cloned.1.call-start = ((), (), s32[]{:S(2)}) async-start(), calls=%async_computation.7 | async-start | bytes 1966080 | tf_op jit(solution)/shard_map/all_gather | solution.py:151
  10.5 4.5 %copy-start.3 = (bf16[96,2048]{1,0:T(8,128)(2,1)S(1)}, bf16[96,2048]{1,0:T(8,128)(2,1)}, u32[]{:S(2)}) copy-start(bf16[96,2048]{1,0:T(8,128)(2,1)} %fusion.54) | copy-start | bytes 1179652
  10.5 251.2 %all-gather.3.cloned.1.call-start = ((), (), s32[]{:S(2)}) async-start(), calls=%async_computation.6 | async-start | bytes 8652800 | tf_op jit(solution)/shard_map/all_gather | solution.py:20
  106.4 5.2 %copy-start.11 = (bf16[2,2048,256]{2,1,0:T(8,128)(2,1)S(1)}, bf16[2,2048,256]{2,1,0:T(8,128)(2,1)}, u32[]{:S(2)}) copy-start(bf16[2,2048,256]{2,1,0:T(8,128)(2,1)} %param.29) | copy-start | bytes 6291460
  109.6 1.9 copy-start.2
  142.9 5.1 %copy-start.13 = (bf16[2048,256]{1,0:T(8,128)(2,1)S(1)}, bf16[2048,256]{1,0:T(8,128)(2,1)}, u32[]{:S(2)}) copy-start(bf16[2048,256]{1,0:T(8,128)(2,1)} %param.32) | copy-start | bytes 3145732
  142.9 53.0 %all-to-all-start.3 = ((bf16[4,256,2048]{2,1,0:T(8,128)(2,1)}), bf16[4,256,2048]{2,1,0:T(8,128)(2,1)}, u32[]{:S(2)}, u32[]{:S(2)}) async-start(bf16[4,256,2048]{2,1,0:T(8,128)(2,1)} %bitcast.108), calls=%async_computation.3 | async-start | bytes 8388608 | tf_op jit(solution)/shard_map/all_to_all | solution.py:31
  148.0 2.1 copy-start.12
  195.9 22.5 %all-to-all-start.5 = ((bf16[4,96,2048]{2,1,0:T(8,128)(2,1)}), bf16[4,96,2048]{2,1,0:T(8,128)(2,1)S(1)}, u32[]{:S(2)}, u32[]{:S(2)}) async-start(bf16[4,96,2048]{2,1,0:T(8,128)(2,1)} %bitcast.112), calls=%async_computation.5 | async-start | bytes 3145728 | tf_op jit(solution)/shard_map/all_to_all | solution.py:31
  202.6 26.0 %copy-start.6 = (bf16[128,256]{1,0:T(8,128)(2,1)S(1)}, bf16[128,256]{1,0:T(8,128)(2,1)}, u32[]{:S(2)}) copy-start(bf16[128,256]{1,0:T(8,128)(2,1)} %param.19) | copy-start | bytes 196612
  202.6 26.4 %copy-start.10 = (f32[96,2]{0,1:T(2,128)S(1)}, f32[96,2]{0,1:T(2,128)}, u32[]{:S(2)}) copy-start(f32[96,2]{0,1:T(2,128)} %param.28) | copy-start | bytes 2308
  218.4 35.1 %all-to-all-start.4 = ((bf16[128,2,2048]{2,1,0:T(2,128)(2,1)}), bf16[128,2,2048]{2,1,0:T(2,128)(2,1)S(1)}, u32[]{:S(2)}, u32[]{:S(2)}) async-start(bf16[128,2,2048]{2,1,0:T(2,128)(2,1)} %reshape.144), calls=%async_computation.4 | async-start | bytes 2097152 | tf_op jit(solution)/shard_map/all_to_all | solution.py:172
  256.0 4.5 %copy-start.5 = (f32[96,2048]{1,0:T(8,128)S(1)}, f32[96,2048]{1,0:T(8,128)}, u32[]{:S(2)}) copy-start(f32[96,2048]{1,0:T(8,128)} %convert_reduce_fusion) | copy-start | bytes 2359300
  261.7 5.9 %slice-start = ((bf16[8192,516]{0,1:T(8,128)(2,1)}), bf16[8192,4]{0,1:T(4,128)(2,1)S(1)}, s32[]{:S(2)}) async-start(bf16[8192,516]{0,1:T(8,128)(2,1)} %all-gather.3.cloned.1.call-done), calls=%async_computation.8 | async-start | bytes 131072 | tf_op jit(solution)/shard_map/split | solution.py:21
  418.4 6.0 %copy-start.4 = (f32[96,2048]{1,0:T(8,128)S(1)}, f32[96,2048]{1,0:T(8,128)}, u32[]{:S(2)}) copy-start(f32[96,2048]{1,0:T(8,128)} %get-tuple-element.101) | copy-start | bytes 2359300
  418.4 6.0 %copy-start.7 = (f32[2048]{0:T(1024)S(1)}, f32[2048]{0:T(1024)}, u32[]{:S(2)}) copy-start(f32[2048]{0:T(1024)} %param.35) | copy-start | bytes 24580
  418.4 16.2 %copy-start.8 = (f32[2048]{0:T(1024)S(1)}, f32[2048]{0:T(1024)}, u32[]{:S(2)}) copy-start(f32[2048]{0:T(1024)} %param.24) | copy-start | bytes 24580
  418.4 17.0 %copy-start.1 = (bf16[2,256,2048]{2,1,0:T(8,128)(2,1)S(1)}, bf16[2,256,2048]{2,1,0:T(8,128)(2,1)}, u32[]{:S(2)}) copy-start(bf16[2,256,2048]{2,1,0:T(8,128)(2,1)} %param.31) | copy-start | bytes 6291460
  421.0 13.5 %all-to-all-start = ((bf16[4,32,2048]{2,1,0:T(8,128)(2,1)}), bf16[4,32,2048]{2,1,0:T(8,128)(2,1)S(1)}, u32[]{:S(2)}, u32[]{:S(2)}) async-start(bf16[4,32,2048]{2,1,0:T(8,128)(2,1)} %bitcast.2), calls=%async_computation | async-start | bytes 1048576 | tf_op jit(solution)/shard_map/all_to_all | solution.py:31
Sparse Core Ops, SparseCore 0:
  10.6 29.1 all-gather.4
  42.4 85.3 all-gather.2
